TPU v7x, 32 devices: a whole 2x2x4 slice. The times are simulated.
32 devices in a mesh: sp: 16 (over z, y, x), tp: 2 (over core).
Axes of the slice: x: 2, y: 2, z: 4, core: 2. Of those that a mesh axis runs over, the one named last changes fastest.
Arguments:
- tokens: bfloat16 [8192, 2048], P('sp', 'tp'), may hold values from -6 to 6
- norm_gain: float32 [2048], replicated, may hold values from 0.1 to 1.9
- outer_gate: bfloat16 [2048, 1024], P('sp', 'tp'), may hold values from -0.125 to 0.125
- inner_gate: bfloat16 [2048, 1024], P('sp', 'tp'), may hold values from -0.125 to 0.125
- conv_input: bfloat16 [2048, 1024], P('sp', 'tp'), may hold values from -0.125 to 0.125
- query_proj: bfloat16 [2048, 1024], P('sp', 'tp'), may hold values from -0.125 to 0.125
- key_proj: bfloat16 [2048, 1024], P('sp', 'tp'), may hold values from -0.125 to 0.125
- value_proj: bfloat16 [2048, 1024], P('sp', 'tp'), may hold values from -0.125 to 0.125
- out_gate: bfloat16 [2048, 1024], P('sp', 'tp'), may hold values from -0.125 to 0.125
- conv_taps: float32 [3, 1024], P(None, 'tp'), may hold values from -3.5 to 3.5
- log_decay: float32 [2, 16, 8192], P(None, 'tp', 'sp'), may hold values from -1.2 to 0, as said below
- head_gain: float32 [1024], P('tp'), may hold values from 0.1 to 1.9
- conv_output: bfloat16 [1024, 2048], P('tp', 'sp'), may hold values from -0.1875 to 0.1875
- retention_output: bfloat16 [1024, 2048], P('tp', 'sp'), may hold values from -0.1875 to 0.1875
Outputs:
- mixed: bfloat16 [8192, 2048], P(('sp', 'tp'))
Inputs may be any that keep to these rules, and one draw needn't show every extreme that they name: `log_decay`: logarithms of per-position decays, below zero.
All inputs are finite; a program needn't handle non-finite values.
Results may differ from a plain program's by a relative error of at most 0.02.
Values may be sent and summed in bfloat16 or wider, within the bound.
A program may use at most 128 MiB of HBM per device.

v0:
```python
import jax
import jax.numpy as jnp
from jax import lax
from jax.sharding import PartitionSpec as P

HEAD_DIM = 64
EPS = 1e-06
THETA = 10000.0


def with_halo(shard, sides, width):
    for axis, dim in sides:
        size, length = (lax.axis_size(axis), shard.shape[dim])
        up = [(i, (i + 1) % size) for i in range(size - 1)]
        down = [(j, i) for i, j in up]
        last = lax.slice_in_dim(shard, length - width, length, axis=dim)
        first = lax.slice_in_dim(shard, 0, width, axis=dim)
        before = lax.ppermute(last, axis, up)
        after = lax.ppermute(first, axis, down)
        shard = jnp.concatenate([before, shard, after], axis=dim)
    return shard


def rotate(field_in, position_list):
    half_dim = field_in.shape[-1] // 2
    frequency = jnp.exp(
        -jnp.log(THETA) * jnp.arange(half_dim, dtype=jnp.float32) * (2.0 / field_in.shape[-1])
    )
    angles = position_list.astype(jnp.float32)[:, None, None] * frequency
    cosine = jnp.cos(angles)
    sine_part = jnp.sin(angles)
    leading = field_in[..., :half_dim]
    trailing = field_in[..., half_dim:]
    return jnp.concatenate(
        [leading * cosine - trailing * sine_part, leading * sine_part + trailing * cosine], axis=-1
    )


def conv_branch(outer_rows, inner_rows, conv_values, conv_taps):
    inner_value = (inner_rows.astype(jnp.float32) * conv_values.astype(jnp.float32)).astype(
        jnp.bfloat16
    )
    padded = with_halo(inner_value, (("sp", 0),), 1).astype(jnp.float32)
    convolved = conv_taps[0] * padded[:-2] + conv_taps[1] * padded[1:-1] + conv_taps[2] * padded[2:]
    return (outer_rows.astype(jnp.float32) * convolved).astype(jnp.bfloat16)


def span_parts(query_rows, key_rows, value_rows, log_rates):
    length = query_rows.shape[0]
    forward_cum = jnp.cumsum(log_rates[0], axis=-1)
    backward_cum = jnp.flip(jnp.cumsum(jnp.flip(log_rates[1], -1), axis=-1), -1)
    row_index = lax.broadcasted_iota(jnp.int32, (length, length), 0)
    col_index = lax.broadcasted_iota(jnp.int32, (length, length), 1)
    lower_part = (col_index <= row_index)[None]
    spread = jnp.where(
        lower_part,
        forward_cum[:, :, None] - forward_cum[:, None, :],
        backward_cum[:, :, None] - backward_cum[:, None, :],
    )
    scores = jnp.einsum("ihe,jhe->hij", query_rows, key_rows, preferred_element_type=jnp.float32)
    weighted = (scores * jnp.exp(spread)).astype(jnp.bfloat16)
    local_part = jnp.einsum(
        "hij,jhe->ihe", weighted, value_rows, preferred_element_type=jnp.float32
    )
    key_wide = key_rows.astype(jnp.float32)
    forward_keys = (key_wide * jnp.exp(forward_cum[:, -1:] - forward_cum).T[:, :, None]).astype(
        jnp.bfloat16
    )
    backward_keys = (key_wide * jnp.exp(backward_cum[:, :1] - backward_cum).T[:, :, None]).astype(
        jnp.bfloat16
    )
    forward_state = jnp.einsum(
        "jhd,jhe->hde", forward_keys, value_rows, preferred_element_type=jnp.float32
    )
    backward_state = jnp.einsum(
        "jhd,jhe->hde", backward_keys, value_rows, preferred_element_type=jnp.float32
    )
    return (local_part, forward_cum, backward_cum, forward_state, backward_state)


def retention_branch(query_rows, key_rows, value_rows, gate_rows, log_decay, head_gain, offsets):
    row_count = query_rows.shape[0]
    head_count = query_rows.shape[1] // HEAD_DIM
    shape_heads = (row_count, head_count, HEAD_DIM)
    rotated_query = rotate(query_rows.astype(jnp.float32).reshape(shape_heads), offsets).astype(
        jnp.bfloat16
    )
    rotated_key = (
        rotate(key_rows.astype(jnp.float32).reshape(shape_heads), offsets) * HEAD_DIM ** (-0.5)
    ).astype(jnp.bfloat16)
    local_part, forward_cum, backward_cum, forward_state, backward_state = span_parts(
        rotated_query, rotated_key, value_rows.reshape(shape_heads), log_decay
    )
    forward_total = forward_cum[:, -1]
    backward_total = backward_cum[:, 0]
    totals = lax.all_gather(
        jnp.stack([forward_total, backward_total])[None], "sp", axis=0, tiled=True
    )
    inclusive = jnp.cumsum(totals, axis=0)
    exclusive = inclusive - totals
    own_index = lax.axis_index("sp")
    own_inclusive = lax.dynamic_index_in_dim(inclusive, own_index, 0, keepdims=False)
    own_exclusive = lax.dynamic_index_in_dim(exclusive, own_index, 0, keepdims=False)
    pieces = (
        lax.all_gather(forward_state[None], "sp", axis=0, tiled=True),
        lax.all_gather(backward_state[None], "sp", axis=0, tiled=True),
    )
    piece_count = pieces[0].shape[0]
    span_index = lax.iota(jnp.int32, piece_count)
    forward_weight = jnp.where(
        (span_index < own_index)[:, None],
        jnp.exp(jnp.minimum(own_exclusive[0] - inclusive[:, 0], 0.0)),
        0.0,
    )
    backward_weight = jnp.where(
        (span_index > own_index)[:, None],
        jnp.exp(jnp.minimum(exclusive[:, 1] - own_inclusive[1], 0.0)),
        0.0,
    )
    into_forward = jnp.einsum(
        "nh,nhde->hde", forward_weight, pieces[0], precision=lax.Precision.HIGHEST
    )
    into_backward = jnp.einsum(
        "nh,nhde->hde", backward_weight, pieces[1], precision=lax.Precision.HIGHEST
    )
    forward_part = jnp.einsum(
        "ihd,hde->ihe",
        rotated_query,
        into_forward.astype(jnp.bfloat16),
        preferred_element_type=jnp.float32,
    )
    backward_part = jnp.einsum(
        "ihd,hde->ihe",
        rotated_query,
        into_backward.astype(jnp.bfloat16),
        preferred_element_type=jnp.float32,
    )
    mixed_heads = (
        local_part
        + jnp.exp(forward_cum).T[:, :, None] * forward_part
        + jnp.exp(backward_cum).T[:, :, None] * backward_part
    )
    scaled = mixed_heads * lax.rsqrt(
        jnp.mean(mixed_heads * mixed_heads, axis=-1, keepdims=True) + EPS
    )
    scaled = scaled * head_gain.reshape(head_count, HEAD_DIM)
    return (
        jax.nn.silu(gate_rows.astype(jnp.float32))
        * scaled.reshape(row_count, head_count * HEAD_DIM)
    ).astype(jnp.bfloat16)


def local(
    tokens,
    norm_gain,
    outer_gate,
    inner_gate,
    conv_input,
    query_proj,
    key_proj,
    value_proj,
    out_gate,
    conv_taps,
    log_decay,
    head_gain,
    conv_output,
    retention_output,
):
    whole = lax.all_gather(tokens, "tp", axis=1, tiled=True)
    wide = whole.astype(jnp.float32)
    normed = (
        wide * lax.rsqrt(jnp.mean(wide * wide, axis=-1, keepdims=True) + EPS) * norm_gain
    ).astype(jnp.bfloat16)
    row_count = normed.shape[0]
    offsets = lax.axis_index("sp") * row_count + lax.iota(jnp.int32, row_count)
    gathered = (
        lax.all_gather(outer_gate, "sp", axis=0, tiled=True),
        lax.all_gather(inner_gate, "sp", axis=0, tiled=True),
        lax.all_gather(conv_input, "sp", axis=0, tiled=True),
        lax.all_gather(query_proj, "sp", axis=0, tiled=True),
        lax.all_gather(key_proj, "sp", axis=0, tiled=True),
        lax.all_gather(value_proj, "sp", axis=0, tiled=True),
        lax.all_gather(out_gate, "sp", axis=0, tiled=True),
        lax.all_gather(conv_output, "sp", axis=1, tiled=True),
        lax.all_gather(retention_output, "sp", axis=1, tiled=True),
    )
    projected = [
        jnp.dot(normed, weight, preferred_element_type=jnp.float32).astype(jnp.bfloat16)
        for weight in gathered[:7]
    ]
    conv_out = conv_branch(projected[0], projected[1], projected[2], conv_taps)
    ret_out = retention_branch(
        projected[3], projected[4], projected[5], projected[6], log_decay, head_gain, offsets
    )
    conv_weight = gathered[7]
    ret_weight = gathered[8]
    return lax.psum_scatter(
        (
            jnp.dot(conv_out, conv_weight, preferred_element_type=jnp.float32)
            + jnp.dot(ret_out, ret_weight, preferred_element_type=jnp.float32)
        ).astype(jnp.bfloat16),
        "tp",
        scatter_dimension=0,
        tiled=True,
    )


def solution(mesh):
    return jax.shard_map(
        local,
        mesh=mesh,
        in_specs=(
            P("sp", "tp"),
            P(),
            P("sp", "tp"),
            P("sp", "tp"),
            P("sp", "tp"),
            P("sp", "tp"),
            P("sp", "tp"),
            P("sp", "tp"),
            P("sp", "tp"),
            P(None, "tp"),
            P(None, "tp", "sp"),
            P("tp"),
            P("tp", "sp"),
            P("tp", "sp"),
        ),
        out_specs=P(("sp", "tp"), None),
        check_vma=False,
    )
```

profile of v0, /device:TPU:0, one launch (start us, length us, event | category | flops | bytes accessed | tf_op | source)
XLA Modules:
  0.0 762.5 jit_solution(9898685039781030391)
XLA Ops:
  14.8 7.4 all-gather.17.cloned.1.call-done
  24.4 62.1 %all-gather.31.cloned.1.call-done = bf16[2048,512]{1,0:T(8,128)(2,1)} async-done(((bf16[128,512]{1,0:T(8,128)(2,1)}), bf16[2048,512]{1,0:T(8,128)(2,1)}) %all-gather.31.cloned.1.call-update) | async-done | bytes 2097168 | tf_op jit(solution)/shard_map/all_gather | solution.py:180
  89.7 58.9 %all-gather.33.cloned.1.call-done = bf16[2048,512]{1,0:T(8,128)(2,1)} async-done(((bf16[128,512]{1,0:T(8,128)(2,1)}), bf16[2048,512]{1,0:T(8,128)(2,1)}) %all-gather.33.cloned.1.call-update) | async-done | bytes 2097168 | tf_op jit(solution)/shard_map/all_gather | solution.py:181
  148.6 3.6 convolution_convert_fusion
  153.4 56.9 %all-gather.29.cloned.1.call-done = bf16[2048,512]{1,0:T(8,128)(2,1)} async-done(((bf16[128,512]{1,0:T(8,128)(2,1)}), bf16[2048,512]{1,0:T(8,128)(2,1)}) %all-gather.29.cloned.1.call-update) | async-done | bytes 2097168 | tf_op jit(solution)/shard_map/all_gather | solution.py:182
  210.4 3.6 convolution_convert_fusion.2
  221.9 38.7 %all-gather.3 = f32[16,2,8]{2,1,0:T(2,128)S(1)} all-gather(f32[1,2,8]{2,1,0:T(2,128)S(1)} %maximum_bitcast_fusion), channel_id=2, replica_groups=mesh['sp'=16,'tp'=2] {'sp'}, dimensions={0}, use_global_device_ids=true | all-gather | bytes 1088 | tf_op jit(solution)/shard_map/all_gather | solution.py:96
  261.0 11.3 %all-gather.21.cloned.1.call-done = bf16[2048,512]{1,0:T(8,128)(2,1)} async-done(((bf16[128,512]{1,0:T(8,128)(2,1)}), bf16[2048,512]{1,0:T(8,128)(2,1)}) %all-gather.21.cloned.1.call-update) | async-done | bytes 2097168 | tf_op jit(solution)/shard_map/all_gather | solution.py:178
  272.3 3.9 fusion.18
  276.2 58.0 %all-gather.23.cloned.1.call-done = bf16[2048,512]{1,0:T(8,128)(2,1)} async-done(((bf16[128,512]{1,0:T(8,128)(2,1)}), bf16[2048,512]{1,0:T(8,128)(2,1)}) %all-gather.23.cloned.1.call-update) | async-done | bytes 2097168 | tf_op jit(solution)/shard_map/all_gather | solution.py:179
  334.2 3.2 fusion.22
  337.4 3.2 collective-permute-start
  342.0 5.8 fusion.11
  349.0 47.2 %all-gather.19.cloned.1.call-done = bf16[2048,512]{1,0:T(8,128)(2,1)} async-done(((bf16[128,512]{1,0:T(8,128)(2,1)}), bf16[2048,512]{1,0:T(8,128)(2,1)}) %all-gather.19.cloned.1.call-update) | async-done | bytes 2097168 | tf_op jit(solution)/shard_map/all_gather | solution.py:177
  396.2 64.5 %all-gather.25.cloned.1.call-done = bf16[512,2048]{1,0:T(8,128)(2,1)} async-done(((bf16[512,128]{1,0:T(8,128)(2,1)}), bf16[512,2048]{1,0:T(8,128)(2,1)}) %all-gather.25.cloned.1.call-update) | async-done | bytes 2097168 | tf_op jit(solution)/shard_map/all_gather | solution.py:184
  460.7 7.7 %fusion.33 = f32[512,2048]{1,0:T(8,128)} fusion(bf16[512,2048]{1,0:T(8,128)(2,1)} %all-gather.25.cloned.1.call-done, bf16[2048,512]{1,0:T(8,128)(2,1)} %all-gather.19.cloned.1.call-done, f32[514,512]{1,0:T(8,128)} %maximum_convert_fusion, f32[512]{0:T(512)S(1)} %bitcast.107, f32[512]{0:T(512)S(1)} %bitcast.108, f32[512]{0:T(512)S(1)} %bitcast.106, ...), kind=kOutput, calls=%fused_computation.56 | convolution fusion | flops 2154037248 | bytes 13647872 | tf_op jit(solution)/shard_map/dot_general | solution.py:199
  468.4 68.8 %all-gather.37.cloned.1.call-done = f32[128,64,64]{2,1,0:T(8,128)} async-done(((f32[8,64,64]{2,1,0:T(8,128)}), f32[128,64,64]{2,1,0:T(8,128)}) %all-gather.37.cloned.1.call-update) | async-done | bytes 2097168 | tf_op jit(solution)/shard_map/all_gather | solution.py:105
  537.2 6.4 fusion.5
  543.8 70.3 %all-gather.39.cloned.1.call-done = f32[128,64,64]{2,1,0:T(8,128)} async-done(((f32[8,64,64]{2,1,0:T(8,128)}), f32[128,64,64]{2,1,0:T(8,128)}) %all-gather.39.cloned.1.call-update) | async-done | bytes 2097168 | tf_op jit(solution)/shard_map/all_gather | solution.py:106
  614.1 6.6 fusion.3
  624.2 51.7 %all-gather.27.cloned.1.call-done = bf16[2048,512]{1,0:T(8,128)(2,1)} async-done(((bf16[128,512]{1,0:T(8,128)(2,1)}), bf16[2048,512]{1,0:T(8,128)(2,1)}) %all-gather.27.cloned.1.call-update) | async-done | bytes 2097168 | tf_op jit(solution)/shard_map/all_gather | solution.py:183
  675.9 64.3 %all-gather.35.cloned.1.call-done = bf16[512,2048]{1,0:T(8,128)(2,1)} async-done(((bf16[512,128]{1,0:T(8,128)(2,1)}), bf16[512,2048]{1,0:T(8,128)(2,1)}) %all-gather.35.cloned.1.call-update) | async-done | bytes 2097168 | tf_op jit(solution)/shard_map/all_gather | solution.py:185
  740.2 7.6 %add_convert_fusion = bf16[512,2048]{1,0:T(8,128)(2,1)} fusion(f32[512,2048]{1,0:T(8,128)} %fusion.33, bf16[512,2048]{1,0:T(8,128)(2,1)} %all-gather.35.cloned.1.call-done, f32[512,512]{1,0:T(8,128)} %copy.34, bf16[2048,512]{1,0:T(8,128)(2,1)} %all-gather.27.cloned.1.call-done, bf16[512,2048]{1,0:T(8,128)(2,1)S(1)} %copy-done.1, f32[2048]{0:T(1024)S(1)} %copy-done.6, ...), kind=kOutput, calls=%fused_computation.10 | convolution fusion | flops 2155872256 | bytes 13641728 | tf_op jit(solution)/shard_map/dot_general | solution.py:200
  747.9 8.1 %reduce-scatter.2.cloned.1.call-done = bf16[256,2048]{1,0:T(8,128)(2,1)} async-done(((bf16[512,2048]{1,0:T(8,128)(2,1)}), bf16[256,2048]{1,0:T(8,128)(2,1)}) %reduce-scatter.2.cloned.1.call-update) | async-done | bytes 1048592 | tf_op jit(solution)/shard_map/reduce_scatter | solution.py:197
  (98 shorter events, 29.2 us)
Async XLA Ops:
  6.5 80.0 %copy-start.6 = (f32[2048]{0:T(1024)S(1)}, f32[2048]{0:T(1024)}, u32[]{:S(2)}) copy-start(f32[2048]{0:T(1024)} %param.15) | copy-start | bytes 24580
  6.5 15.7 %all-gather.17.cloned.1.call-start = ((), (), s32[]{:S(2)}) async-start(), calls=%async_computation.1 | async-start | bytes 3145728 | tf_op jit(solution)/shard_map/all_gather | solution.py:169
  7.3 79.3 %all-gather.31.cloned.1.call-start = ((), (), s32[]{:S(2)}) async-start(), calls=%async_computation.8 | async-start | bytes 2228224 | tf_op jit(solution)/shard_map/all_gather | solution.py:180
  8.0 140.5 %all-gather.33.cloned.1.call-start = ((), (), s32[]{:S(2)}) async-start(), calls=%async_computation.9 | async-start | bytes 2228224 | tf_op jit(solution)/shard_map/all_gather | solution.py:181
  8.7 201.6 %all-gather.29.cloned.1.call-start = ((), (), s32[]{:S(2)}) async-start(), calls=%async_computation.7 | async-start | bytes 2228224 | tf_op jit(solution)/shard_map/all_gather | solution.py:182
  9.3 263.0 %all-gather.21.cloned.1.call-start = ((), (), s32[]{:S(2)}) async-start(), calls=%async_computation.3 | async-start | bytes 2228224 | tf_op jit(solution)/shard_map/all_gather | solution.py:178
  9.9 324.3 %all-gather.23.cloned.1.call-start = ((), (), s32[]{:S(2)}) async-start(), calls=%async_computation.4 | async-start | bytes 2228224 | tf_op jit(solution)/shard_map/all_gather | solution.py:179
  10.5 385.7 %all-gather.19.cloned.1.call-start = ((), (), s32[]{:S(2)}) async-start(), calls=%async_computation.2 | async-start | bytes 2228224 | tf_op jit(solution)/shard_map/all_gather | solution.py:177
  11.2 449.4 %all-gather.25.cloned.1.call-start = ((), (), s32[]{:S(2)}) async-start(), calls=%async_computation.5 | async-start | bytes 2228224 | tf_op jit(solution)/shard_map/all_gather | solution.py:184
  12.0 525.3 %all-gather.37.cloned.1.call-start = ((), (), s32[]{:S(2)}) async-start(), calls=%async_computation.12 | async-start | bytes 4456448 | tf_op jit(solution)/shard_map/all_gather | solution.py:105
  22.2 64.4 %copy-start = (bf16[512,2048]{1,0:T(8,128)(2,1)S(1)}, bf16[512,2048]{1,0:T(8,128)(2,1)}, u32[]{:S(2)}) copy-start(bf16[512,2048]{1,0:T(8,128)(2,1)} %all-gather.17.cloned.1.call-done) | copy-start | bytes 6291460
  153.4 64.7 %copy-start.2 = (f32[512,8,32]{0,2,1:T(8,128)}, f32[512,8,32]{0,2,1:T(8,128)S(1)}, u32[]{:S(2)}) copy-start(f32[512,8,32]{0,2,1:T(8,128)S(1)} %get-tuple-element.7) | copy-start | bytes 1572868
  153.4 61.3 %copy-start.3 = (f32[512,8,32]{0,2,1:T(8,128)S(1)}, f32[512,8,32]{0,2,1:T(8,128)}, u32[]{:S(2)}) copy-start(f32[512,8,32]{0,2,1:T(8,128)} %get-tuple-element.8) | copy-start | bytes 1572868
  214.0 0.8 copy-start.7
  215.8 45.0 %copy-start.5 = (f32[512]{0:T(512)S(1)}, f32[512]{0:T(512)}, u32[]{:S(2)}) copy-start(f32[512]{0:T(512)} %param.25) | copy-start | bytes 6148
  215.8 45.1 %copy-start.4 = (f32[3,512]{1,0:T(4,128)S(1)}, f32[3,512]{1,0:T(4,128)}, u32[]{:S(2)}) copy-start(f32[3,512]{1,0:T(4,128)} %param.23) | copy-start | bytes 18436
  215.8 56.5 %copy-start.1 = (bf16[512,2048]{1,0:T(8,128)(2,1)S(1)}, bf16[512,2048]{1,0:T(8,128)(2,1)}, u32[]{:S(2)}) copy-start(bf16[512,2048]{1,0:T(8,128)(2,1)} %all-gather.17.cloned.1.call-done) | copy-start | bytes 6291460
  215.8 398.2 %all-gather.39.cloned.1.call-start = ((), (), s32[]{:S(2)}) async-start(), calls=%async_computation.13 | async-start | bytes 4456448 | tf_op jit(solution)/shard_map/all_gather | solution.py:106
  220.4 455.5 %all-gather.27.cloned.1.call-start = ((), (), s32[]{:S(2)}) async-start(), calls=%async_computation.6 | async-start | bytes 2228224 | tf_op jit(solution)/shard_map/all_gather | solution.py:183
  221.1 519.1 %all-gather.35.cloned.1.call-start = ((), (), s32[]{:S(2)}) async-start(), calls=%async_computation.10 | async-start | bytes 2228224 | tf_op jit(solution)/shard_map/all_gather | solution.py:185
  221.7 534.2 %reduce-scatter.2.cloned.1.call-start = ((), (), s32[]{:S(2)}) async-start(), calls=%async_computation.11 | async-start | bytes 3145728 | tf_op jit(solution)/shard_map/reduce_scatter | solution.py:197
  337.4 10.4 %collective-permute-start = (bf16[1,512]{1,0:T(2,128)(2,1)S(1)}, bf16[1,512]{1,0:T(2,128)(2,1)S(1)}, u32[]{:S(2)}, u32[]{:S(2)}) collective-permute-start(bf16[1,512]{1,0:T(2,128)(2,1)S(1)} %get-tuple-element.11), channel_id=1, source_target_pairs={{0,2},{2,4},{4,6},{6,8},{8,10},{10,12},{12,14},{14,16},{16,18},{18... | collective-permute-start | bytes 3080 | tf_op jit(solution)/shard_map/ppermute | solution.py:18
  340.5 7.3 collective-permute-start.1
Sparse Core Ops, SparseCore 0:
  8.9 13.2 all-gather.16
  25.0 61.5 all-gather.30
  89.3 59.1 all-gather.32
  151.2 59.1 all-gather.28
  213.0 59.2 all-gather.20
  275.0 59.1 all-gather.22
  336.9 59.1 all-gather.18
  398.9 61.7 all-gather.24
  463.4 73.7 all-gather.36
  539.9 74.1 all-gather.38
  616.9 58.9 all-gather.26
  678.4 61.7 all-gather.34
  748.0 7.9 reduce-scatter.1
where the time goes:
time: 763 us; the launch traced here: 762 us
  waiting for transfers between devices  636 us (83%)
  matrix products  56.5 us (7%)
  blocking collectives  38.7 us (5%)
  between operations  13.5 us (2%)
  other arithmetic  8.18 us (1%)
    all_gather x1, waiting for transfers between devices, retention_branch(): lax.all_gather(backward_state[None], 'sp', axis=0, tiled=True)  70.3 us
    all_gather x1, waiting for transfers between devices, retention_branch(): lax.all_gather(forward_state[None], 'sp', axis=0, tiled=True)  68.8 us
    all_gather x1, waiting for transfers between devices, local(): lax.all_gather(conv_output, 'sp', axis=1, tiled=True)  64.5 us
    all_gather x1, waiting for transfers between devices, local(): lax.all_gather(retention_output, 'sp', axis=1, tiled=True)  64.3 us
    all_gather x1, waiting for transfers between devices, local(): lax.all_gather(query_proj, 'sp', axis=0, tiled=True)  62.1 us
    all_gather x1, waiting for transfers between devices, local(): lax.all_gather(key_proj, 'sp', axis=0, tiled=True)  58.9 us
    all_gather x1, waiting for transfers between devices, local(): lax.all_gather(conv_input, 'sp', axis=0, tiled=True)  58 us
    all_gather x1, waiting for transfers between devices, local(): lax.all_gather(value_proj, 'sp', axis=0, tiled=True)  56.9 us
  transfers between devices with their start and end apart: 15, of which 13 were waited for; matrix products, arithmetic and copies ran while one was open for 8% of the time, Pallas kernels for 0%

commit v1 on v0

--- a/solution.py
+++ b/solution.py
@@ -6,6 +6,12 @@
 HEAD_DIM = 64
 EPS = 1e-06
 THETA = 10000.0
+
+
+def gather_blocks(block, name, dim):
+    parts = lax.all_gather(block, name, axis=0, tiled=False)
+    result = jnp.concatenate(parts, axis=dim)
+    return result
 
 
 def with_halo(shard, sides, width):
@@ -182,7 +188,7 @@
         lax.all_gather(value_proj, "sp", axis=0, tiled=True),
         lax.all_gather(out_gate, "sp", axis=0, tiled=True),
         lax.all_gather(conv_output, "sp", axis=1, tiled=True),
-        lax.all_gather(retention_output, "sp", axis=1, tiled=True),
+        gather_blocks(retention_output, "sp", 1),
     )
     projected = [
         jnp.dot(normed, weight, preferred_element_type=jnp.float32).astype(jnp.bfloat16)

time: 763 us -> 761 us (level)
    all_gather x1, waiting for transfers between devices: 64.3 us -> 48.4 us  [gather_blocks(): parts = lax.all_gather(block, name, axis=0, tiled=False)]
    all_gather x1, waiting for transfers between devices: 47.2 us -> 56.9 us  [local(): lax.all_gather(outer_gate, 'sp', axis=0, tiled=True)]
where the time goes in v1:
time: 761 us; the launch traced here: 760 us
  waiting for transfers between devices  631 us (83%)
  matrix products  56.3 us (7%)
  blocking collectives  38.6 us (5%)
  between operations  13.5 us (2%)
  other arithmetic  8.2 us (1%)
  local copies, waits for them, and re-layouts  7.87 us (1%)
    all_gather x1, waiting for transfers between devices, retention_branch(): lax.all_gather(backward_state[None], 'sp', axis=0, tiled=True)  70.4 us
    all_gather x1, waiting for transfers between devices, retention_branch(): lax.all_gather(forward_state[None], 'sp', axis=0, tiled=True)  68.7 us
    all_gather x1, waiting for transfers between devices, local(): lax.all_gather(conv_output, 'sp', axis=1, tiled=True)  64.5 us
    all_gather x1, waiting for transfers between devices, local(): lax.all_gather(query_proj, 'sp', axis=0, tiled=True)  62.1 us
    all_gather x1, waiting for transfers between devices, local(): lax.all_gather(key_proj, 'sp', axis=0, tiled=True)  58.9 us
    all_gather x1, waiting for transfers between devices, local(): lax.all_gather(conv_input, 'sp', axis=0, tiled=True)  58 us
    all_gather x1, waiting for transfers between devices, local(): lax.all_gather(value_proj, 'sp', axis=0, tiled=True)  56.9 us
    all_gather x1, waiting for transfers between devices, local(): lax.all_gather(outer_gate, 'sp', axis=0, tiled=True)  56.9 us
  transfers between devices with their start and end apart: 15, of which 13 were waited for; matrix products, arithmetic and copies ran while one was open for 8% of the time, Pallas kernels for 0%

profile of v1, /device:TPU:0, one launch (start us, length us, event | category | flops | bytes accessed | tf_op | source)
XLA Modules:
  0.0 760.5 jit_solution(4519337541063496447)
XLA Ops:
  14.8 7.4 all-gather.18.cloned.1.call-done
  24.4 62.1 %all-gather.32.cloned.1.call-done = bf16[2048,512]{1,0:T(8,128)(2,1)} async-done(((bf16[128,512]{1,0:T(8,128)(2,1)}), bf16[2048,512]{1,0:T(8,128)(2,1)}) %all-gather.32.cloned.1.call-update) | async-done | bytes 2097168 | tf_op jit(solution)/shard_map/all_gather | solution.py:186
  89.7 58.9 %all-gather.34.cloned.1.call-done = bf16[2048,512]{1,0:T(8,128)(2,1)} async-done(((bf16[128,512]{1,0:T(8,128)(2,1)}), bf16[2048,512]{1,0:T(8,128)(2,1)}) %all-gather.34.cloned.1.call-update) | async-done | bytes 2097168 | tf_op jit(solution)/shard_map/all_gather | solution.py:187
  148.6 3.6 convolution_convert_fusion
  153.5 56.9 %all-gather.30.cloned.1.call-done = bf16[2048,512]{1,0:T(8,128)(2,1)} async-done(((bf16[128,512]{1,0:T(8,128)(2,1)}), bf16[2048,512]{1,0:T(8,128)(2,1)}) %all-gather.30.cloned.1.call-update) | async-done | bytes 2097168 | tf_op jit(solution)/shard_map/all_gather | solution.py:188
  210.4 3.6 convolution_convert_fusion.2
  221.2 38.6 %all-gather.4 = f32[16,2,8]{2,1,0:T(2,128)S(1)} all-gather(f32[1,2,8]{2,1,0:T(2,128)S(1)} %maximum_bitcast_fusion), channel_id=2, replica_groups=mesh['sp'=16,'tp'=2] {'sp'}, dimensions={0}, use_global_device_ids=true | all-gather | bytes 1088 | tf_op jit(solution)/shard_map/all_gather | solution.py:102
  260.3 11.9 %all-gather.22.cloned.1.call-done = bf16[2048,512]{1,0:T(8,128)(2,1)} async-done(((bf16[128,512]{1,0:T(8,128)(2,1)}), bf16[2048,512]{1,0:T(8,128)(2,1)}) %all-gather.22.cloned.1.call-update) | async-done | bytes 2097168 | tf_op jit(solution)/shard_map/all_gather | solution.py:184
  272.2 3.9 fusion.18
  276.1 58.0 %all-gather.24.cloned.1.call-done = bf16[2048,512]{1,0:T(8,128)(2,1)} async-done(((bf16[128,512]{1,0:T(8,128)(2,1)}), bf16[2048,512]{1,0:T(8,128)(2,1)}) %all-gather.24.cloned.1.call-update) | async-done | bytes 2097168 | tf_op jit(solution)/shard_map/all_gather | solution.py:185
  337.2 3.2 collective-permute-start
  341.9 5.8 fusion.11
  347.6 48.4 %all-gather.40.cloned.1.call-done = bf16[8192,128]{1,0:T(8,128)(2,1)} async-done(((bf16[512,128]{1,0:T(8,128)(2,1)}), bf16[8192,128]{1,0:T(8,128)(2,1)}) %all-gather.40.cloned.1.call-update) | async-done | bytes 2097168 | tf_op jit(solution)/shard_map/all_gather | solution.py:12
  396.0 3.9 copy.36
  401.1 56.9 %all-gather.20.cloned.1.call-done = bf16[2048,512]{1,0:T(8,128)(2,1)} async-done(((bf16[128,512]{1,0:T(8,128)(2,1)}), bf16[2048,512]{1,0:T(8,128)(2,1)}) %all-gather.20.cloned.1.call-update) | async-done | bytes 2097168 | tf_op jit(solution)/shard_map/all_gather | solution.py:183
  458.0 64.5 %all-gather.26.cloned.1.call-done = bf16[512,2048]{1,0:T(8,128)(2,1)} async-done(((bf16[512,128]{1,0:T(8,128)(2,1)}), bf16[512,2048]{1,0:T(8,128)(2,1)}) %all-gather.26.cloned.1.call-update) | async-done | bytes 2097168 | tf_op jit(solution)/shard_map/all_gather | solution.py:190
  522.5 7.7 %fusion.33 = f32[512,2048]{1,0:T(8,128)} fusion(bf16[512,2048]{1,0:T(8,128)(2,1)} %all-gather.26.cloned.1.call-done, bf16[2048,512]{1,0:T(8,128)(2,1)} %all-gather.20.cloned.1.call-done, f32[514,512]{1,0:T(8,128)} %maximum_convert_fusion, f32[512]{0:T(512)S(1)} %bitcast.113, f32[512]{0:T(512)S(1)} %bitcast.114, f32[512]{0:T(512)S(1)} %bitcast.112, ...), kind=kOutput, calls=%fused_computation.56 | convolution fusion | flops 2154037248 | bytes 13647872 | tf_op jit(solution)/shard_map/dot_general | solution.py:205
  530.2 68.7 %all-gather.36.cloned.1.call-done = f32[128,64,64]{2,1,0:T(8,128)} async-done(((f32[8,64,64]{2,1,0:T(8,128)}), f32[128,64,64]{2,1,0:T(8,128)}) %all-gather.36.cloned.1.call-update) | async-done | bytes 2097168 | tf_op jit(solution)/shard_map/all_gather | solution.py:111
  598.9 6.4 fusion.5
  605.5 70.4 %all-gather.38.cloned.1.call-done = f32[128,64,64]{2,1,0:T(8,128)} async-done(((f32[8,64,64]{2,1,0:T(8,128)}), f32[128,64,64]{2,1,0:T(8,128)}) %all-gather.38.cloned.1.call-update) | async-done | bytes 2097168 | tf_op jit(solution)/shard_map/all_gather | solution.py:112
  675.9 6.4 fusion.3
  685.8 51.8 %all-gather.28.cloned.1.call-done = bf16[2048,512]{1,0:T(8,128)(2,1)} async-done(((bf16[128,512]{1,0:T(8,128)(2,1)}), bf16[2048,512]{1,0:T(8,128)(2,1)}) %all-gather.28.cloned.1.call-update) | async-done | bytes 2097168 | tf_op jit(solution)/shard_map/all_gather | solution.py:189
  737.6 7.6 %add_convert_fusion = bf16[512,2048]{1,0:T(8,128)(2,1)} fusion(f32[512,2048]{1,0:T(8,128)} %fusion.33, bf16[512,2048]{0,1:T(8,128)(2,1)} %bitcast.104, f32[512,512]{1,0:T(8,128)} %copy.35, bf16[2048,512]{1,0:T(8,128)(2,1)} %all-gather.28.cloned.1.call-done, bf16[512,2048]{1,0:T(8,128)(2,1)S(1)} %copy-done.1, f32[2048]{0:T(1024)S(1)} %copy-done.7, ...), kind=kOutput, calls=%fused_computation.10 | convolution fusion | flops 2155872256 | bytes 13641728 | tf_op jit(solution)/shard_map/dot_general | solution.py:206
  745.2 8.7 %reduce-scatter.2.cloned.1.call-done = bf16[256,2048]{1,0:T(8,128)(2,1)} async-done(((bf16[512,2048]{1,0:T(8,128)(2,1)}), bf16[256,2048]{1,0:T(8,128)(2,1)}) %reduce-scatter.2.cloned.1.call-update) | async-done | bytes 1048592 | tf_op jit(solution)/shard_map/reduce_scatter | solution.py:203
  (101 shorter events, 31.6 us)
Async XLA Ops:
  6.5 6.2 copy-start.4
  6.5 80.0 %copy-start.7 = (f32[2048]{0:T(1024)S(1)}, f32[2048]{0:T(1024)}, u32[]{:S(2)}) copy-start(f32[2048]{0:T(1024)} %param.15) | copy-start | bytes 24580
  6.5 15.7 %all-gather.18.cloned.1.call-start = ((), (), s32[]{:S(2)}) async-start(), calls=%async_computation.1 | async-start | bytes 3145728 | tf_op jit(solution)/shard_map/all_gather | solution.py:175
  7.3 79.3 %all-gather.32.cloned.1.call-start = ((), (), s32[]{:S(2)}) async-start(), calls=%async_computation.8 | async-start | bytes 2228224 | tf_op jit(solution)/shard_map/all_gather | solution.py:186
  8.0 140.5 %all-gather.34.cloned.1.call-start = ((), (), s32[]{:S(2)}) async-start(), calls=%async_computation.9 | async-start | bytes 2228224 | tf_op jit(solution)/shard_map/all_gather | solution.py:187
  8.7 201.6 %all-gather.30.cloned.1.call-start = ((), (), s32[]{:S(2)}) async-start(), calls=%async_computation.7 | async-start | bytes 2228224 | tf_op jit(solution)/shard_map/all_gather | solution.py:188
  9.3 262.9 %all-gather.22.cloned.1.call-start = ((), (), s32[]{:S(2)}) async-start(), calls=%async_computation.3 | async-start | bytes 2228224 | tf_op jit(solution)/shard_map/all_gather | solution.py:184
  9.9 324.1 %all-gather.24.cloned.1.call-start = ((), (), s32[]{:S(2)}) async-start(), calls=%async_computation.4 | async-start | bytes 2228224 | tf_op jit(solution)/shard_map/all_gather | solution.py:185
  10.5 385.6 %all-gather.40.cloned.1.call-start = ((), (), s32[]{:S(2)}) async-start(), calls=%async_computation.13 | async-start | bytes 2228224 | tf_op jit(solution)/shard_map/all_gather | solution.py:12
  11.2 446.8 %all-gather.20.cloned.1.call-start = ((), (), s32[]{:S(2)}) async-start(), calls=%async_computation.2 | async-start | bytes 2228224 | tf_op jit(solution)/shard_map/all_gather | solution.py:183
  12.0 510.5 %all-gather.26.cloned.1.call-start = ((), (), s32[]{:S(2)}) async-start(), calls=%async_computation.5 | async-start | bytes 2228224 | tf_op jit(solution)/shard_map/all_gather | solution.py:190
  12.7 586.2 %all-gather.36.cloned.1.call-start = ((), (), s32[]{:S(2)}) async-start(), calls=%async_computation.11 | async-start | bytes 4456448 | tf_op jit(solution)/shard_map/all_gather | solution.py:111
  22.2 64.4 %copy-start = (bf16[512,2048]{1,0:T(8,128)(2,1)S(1)}, bf16[512,2048]{1,0:T(8,128)(2,1)}, u32[]{:S(2)}) copy-start(bf16[512,2048]{1,0:T(8,128)(2,1)} %all-gather.18.cloned.1.call-done) | copy-start | bytes 6291460
  153.4 64.7 %copy-start.2 = (f32[512,8,32]{0,2,1:T(8,128)}, f32[512,8,32]{0,2,1:T(8,128)S(1)}, u32[]{:S(2)}) copy-start(f32[512,8,32]{0,2,1:T(8,128)S(1)} %get-tuple-element.7) | copy-start | bytes 1572868
  153.4 61.3 %copy-start.3 = (f32[512,8,32]{0,2,1:T(8,128)S(1)}, f32[512,8,32]{0,2,1:T(8,128)}, u32[]{:S(2)}) copy-start(f32[512,8,32]{0,2,1:T(8,128)} %get-tuple-element.8) | copy-start | bytes 1572868
  214.0 0.8 copy-start.8
  215.8 44.2 %copy-start.6 = (f32[512]{0:T(512)S(1)}, f32[512]{0:T(512)}, u32[]{:S(2)}) copy-start(f32[512]{0:T(512)} %param.25) | copy-start | bytes 6148
  215.8 44.2 %copy-start.5 = (f32[3,512]{1,0:T(4,128)S(1)}, f32[3,512]{1,0:T(4,128)}, u32[]{:S(2)}) copy-start(f32[3,512]{1,0:T(4,128)} %param.23) | copy-start | bytes 18436
  215.8 56.4 %copy-start.1 = (bf16[512,2048]{1,0:T(8,128)(2,1)S(1)}, bf16[512,2048]{1,0:T(8,128)(2,1)}, u32[]{:S(2)}) copy-start(bf16[512,2048]{1,0:T(8,128)(2,1)} %all-gather.18.cloned.1.call-done) | copy-start | bytes 6291460
  215.9 460.1 %all-gather.38.cloned.1.call-start = ((), (), s32[]{:S(2)}) async-start(), calls=%async_computation.12 | async-start | bytes 4456448 | tf_op jit(solution)/shard_map/all_gather | solution.py:112
  220.4 517.1 %all-gather.28.cloned.1.call-start = ((), (), s32[]{:S(2)}) async-start(), calls=%async_computation.6 | async-start | bytes 2228224 | tf_op jit(solution)/shard_map/all_gather | solution.py:189
  221.0 532.9 %reduce-scatter.2.cloned.1.call-start = ((), (), s32[]{:S(2)}) async-start(), calls=%async_computation.10 | async-start | bytes 3145728 | tf_op jit(solution)/shard_map/reduce_scatter | solution.py:203
  337.2 62.7 %collective-permute-start = (bf16[1,512]{1,0:T(2,128)(2,1)S(1)}, bf16[1,512]{1,0:T(2,128)(2,1)S(1)}, u32[]{:S(2)}, u32[]{:S(2)}) collective-permute-start(bf16[1,512]{1,0:T(2,128)(2,1)S(1)} %get-tuple-element.11), channel_id=1, source_target_pairs={{0,2},{2,4},{4,6},{6,8},{8,10},{10,12},{12,14},{14,16},{16,18},{18... | collective-permute-start | bytes 3080 | tf_op jit(solution)/shard_map/ppermute | solution.py:24
  340.4 59.6 %collective-permute-start.1 = (bf16[1,512]{1,0:T(2,128)(2,1)S(1)}, bf16[1,512]{1,0:T(2,128)(2,1)S(1)}, u32[]{:S(2)}, u32[]{:S(2)}) collective-permute-start(bf16[1,512]{1,0:T(2,128)(2,1)S(1)} %get-tuple-element.12), channel_id=1, source_target_pairs={{2,0},{4,2},{6,4},{8,6},{10,8},{12,10},{14,12},{16,14},{18,16},{20... | collective-permute-start | bytes 3080 | tf_op jit(solution)/shard_map/ppermute | solution.py:25
Sparse Core Ops, SparseCore 0:
  8.9 13.2 all-gather.17
  25.0 61.5 all-gather.31
  89.3 59.1 all-gather.33
  151.2 59.1 all-gather.29
  213.0 59.1 all-gather.21
  274.8 59.1 all-gather.23
  336.8 59.1 all-gather.39
  398.8 59.1 all-gather.19
  460.7 61.7 all-gather.25
  525.1 73.7 all-gather.35
  601.7 74.1 all-gather.37
  678.6 58.9 all-gather.27
  745.4 8.5 reduce-scatter.1
